TPU v7x, 32 devices: a whole 2x2x4 slice. The times are simulated.
32 devices in a mesh: ep: 4 (over y, x), tp: 8 (over z, core).
Axes of the slice: x: 2, y: 2, z: 4, core: 2. Of those that a mesh axis runs over, the one named last changes fastest.
Arguments:
- query_rows: bfloat16 [512, 2048], P('ep', 'tp'), may hold values from -32 to 32
- key_rows: bfloat16 [512, 2048], P('ep', 'tp'), may hold values from -8 to 8
- value_rows: bfloat16 [512, 2048], P('ep', 'tp'), may hold values from -8 to 8
- query_norm_gain: float32 [64], replicated, may hold values from 0.1 to 1.9
- key_gain: float32 [64], replicated, may hold values from 0.1 to 1.9
- break_offset: float32 [32], P('tp'), may hold values from -12 to 3
- mixer_out_weight: bfloat16 [2048, 2048], P('tp'), may hold values from -0.75 to 0.75
- routed_tokens: bfloat16 [4096, 2048], P(('ep', 'tp')), may hold values from -6 to 6
- expert_gain: float32 [2048], replicated, may hold values from 0.1 to 1.9
- routes: int32 [4096, 2], P(('ep', 'tp')), may hold values from 0 to 3, as said below
- route_scores: float32 [4096, 2], P(('ep', 'tp')), may hold values from -6 to 6
- gate_weight: bfloat16 [4, 2048, 3584], P('ep', None, 'tp'), may hold values from -0.125 to 0.125
- up_weight: bfloat16 [4, 2048, 3584], P('ep', None, 'tp'), may hold values from -0.125 to 0.125
- down_weight: bfloat16 [4, 3584, 2048], P('ep', 'tp'), may hold values from -0.09375 to 0.09375
Outputs:
- attention_output: bfloat16 [512, 2048], P(('ep', 'tp'))
- expert_output: bfloat16 [4096, 2048], P(('ep', 'tp'))
Inputs may be any that keep to these rules, and one draw needn't show every extreme that they name: `routes`: each row names 2 different experts. Among the rows of one device no expert is named more than 64 times, and one expert is named exactly 64 times by the rows of every device.
All inputs are finite; a program needn't handle non-finite values.
Results may differ from a plain program's by a relative error of at most 0.018.
Values may be sent and summed in bfloat16 or wider, within the bound.
A program may use at most 128 MiB of HBM per device.

v0:
```python
import jax
import jax.numpy as jnp
from jax import lax
from jax.sharding import PartitionSpec as P

HEAD_DIM = 64
TOP_K = 2
EPS = 1e-06


def shifted(array, axis, by):
    peers = lax.axis_size(axis)
    pairs = [(i, i + by) for i in range(peers) if 0 <= i + by < peers]
    return lax.ppermute(array, axis, pairs)


def norm_heads(flat, gain):
    count = flat.shape[0]
    split = flat.astype(jnp.float32).reshape(count, -1, HEAD_DIM)
    scaled = split * lax.rsqrt(jnp.mean(split * split, axis=2, keepdims=True) + EPS)
    return (scaled * gain).astype(jnp.bfloat16)


def absorb(carry_state, query_norm, key_flat, value_flat, offsets, allowed):
    running_sum, carried = carry_state
    key_count = key_flat.shape[0]
    key_norm = key_flat.reshape(key_count, -1, HEAD_DIM)
    value_heads = value_flat.reshape(key_count, -1, HEAD_DIM)
    scores = jnp.einsum("qhd,khd->hqk", query_norm, key_norm, preferred_element_type=jnp.float32)
    scores = scores * HEAD_DIM ** (-0.5) + offsets[:, None, None]
    log_rise = jax.nn.log_sigmoid(scores)
    log_fail = jnp.where(allowed[None], log_rise - scores, 0.0)
    log_after = carried[:, :, None] + lax.cumsum(log_fail, axis=2, reverse=True) - log_fail
    weights = jnp.where(allowed[None], jnp.exp(log_rise + log_after), 0.0).astype(jnp.bfloat16)
    running_sum = running_sum + jnp.einsum(
        "hqk,khd->qhd", weights, value_heads, preferred_element_type=jnp.float32
    )
    return (running_sum, carried + jnp.sum(log_fail, axis=2))


def mixer_reduce(heads_mixed, mixer_out_weight):
    return lax.psum_scatter(
        jnp.dot(heads_mixed, mixer_out_weight, preferred_element_type=jnp.float32).astype(
            jnp.bfloat16
        ),
        "tp",
        scatter_dimension=0,
        tiled=True,
    ).astype(jnp.float32)


def body(
    query_rows,
    key_rows,
    value_rows,
    query_norm_gain,
    key_gain,
    break_offset,
    mixer_out_weight,
    routed_tokens,
    expert_gain,
    routes,
    route_scores,
    gate_weight,
    up_weight,
    down_weight,
):
    gate_local = gate_weight[0]
    up_local = up_weight[0]
    down_local = down_weight[0]
    row_count = query_rows.shape[0]
    query_norm = norm_heads(query_rows, query_norm_gain)
    head_count = query_norm.shape[1]
    key_flat = norm_heads(key_rows, key_gain).reshape(row_count, -1)
    my_index = lax.axis_index("ep")
    devices_ep = lax.axis_size("ep")
    token_position = jnp.arange(row_count)
    earlier = token_position[None, :] < token_position[:, None]
    carry_state = (
        jnp.zeros((row_count, head_count, HEAD_DIM), jnp.float32),
        jnp.zeros((head_count, row_count), jnp.float32),
    )
    carry_state = absorb(carry_state, query_norm, key_flat, value_rows, break_offset, earlier)

    def next_turn(turn_index, loop_carry):
        key_now, value_now, state_now = loop_carry
        key_now, value_now = shifted((key_now, value_now), "ep", 1)
        allowed = jnp.broadcast_to(my_index >= turn_index, (row_count, row_count))
        return (
            key_now,
            value_now,
            absorb(state_now, query_norm, key_now, value_now, break_offset, allowed),
        )

    carry_state = lax.fori_loop(1, devices_ep, next_turn, (key_flat, value_rows, carry_state))[2]
    heads_mixed = carry_state[0].astype(jnp.bfloat16).reshape(row_count, -1)
    token_count = routed_tokens.shape[0]
    model_width = routed_tokens.shape[1]
    as_float = routed_tokens.astype(jnp.float32)
    normed = (
        as_float
        * lax.rsqrt(jnp.mean(as_float * as_float, axis=1, keepdims=True) + EPS)
        * expert_gain
    ).astype(jnp.bfloat16)
    expert_count = lax.axis_size("ep")
    capacity = max(2, token_count * TOP_K // expert_count)
    flat_routes = routes.reshape(-1)
    member = (flat_routes[:, None] == jnp.arange(expert_count, dtype=jnp.int32)[None, :]).astype(
        jnp.int32
    )
    ahead = jnp.sum((jnp.cumsum(member, axis=0) - member) * member, axis=1)
    slot_index = flat_routes * capacity + ahead
    select = (
        slot_index[:, None] == jnp.arange(expert_count * capacity, dtype=jnp.int32)[None, :]
    ).astype(jnp.bfloat16)
    copies = jnp.repeat(normed, TOP_K, axis=0)
    outgoing = jnp.einsum("cs,cd->sd", select, copies, preferred_element_type=jnp.float32).astype(
        jnp.bfloat16
    )
    arrived = lax.all_to_all(outgoing, "ep", split_axis=0, concat_axis=0, tiled=True)
    piece = lax.all_gather(arrived, "tp", axis=0, tiled=True)
    gate_piece = jnp.dot(piece, gate_local, preferred_element_type=jnp.float32)
    up_piece = jnp.dot(piece, up_local, preferred_element_type=jnp.float32)
    hidden = (jax.nn.silu(gate_piece) * up_piece).astype(jnp.bfloat16)
    mixer_sum = mixer_reduce(heads_mixed, mixer_out_weight)
    expert_sum = lax.psum_scatter(
        jnp.dot(hidden, down_local, preferred_element_type=jnp.float32).astype(jnp.bfloat16),
        "tp",
        scatter_dimension=0,
        tiled=True,
    )
    returned = lax.all_to_all(expert_sum, "ep", split_axis=0, concat_axis=0, tiled=True)
    results = jnp.einsum("cs,sd->cd", select, returned, preferred_element_type=jnp.float32)
    results = results.reshape(token_count, TOP_K, model_width)
    differences = route_scores[:, None, :] - route_scores[:, :, None]
    route_weight = 1.0 / jnp.sum(jnp.exp(differences), axis=2)
    expert_output = jnp.sum(route_weight[..., None] * results, axis=1).astype(jnp.bfloat16)
    return (mixer_sum.astype(jnp.bfloat16), expert_output)


def solution(mesh):
    in_specs = (
        P("ep", "tp"),
        P("ep", "tp"),
        P("ep", "tp"),
        P(),
        P(),
        P("tp"),
        P("tp", None),
        P(("ep", "tp"), None),
        P(),
        P(("ep", "tp"), None),
        P(("ep", "tp"), None),
        P("ep", None, "tp"),
        P("ep", None, "tp"),
        P("ep", "tp", None),
    )
    out_specs = (P(("ep", "tp"), None), P(("ep", "tp"), None))
    return jax.shard_map(body, mesh=mesh, in_specs=in_specs, out_specs=out_specs, check_vma=False)
```

profile of v0, /device:TPU:0, one launch (start us, length us, event | category | flops | bytes accessed | tf_op | source)
XLA Modules:
  0.0 263.1 jit_solution(493648359935207742)
XLA Ops:
  7.2 0.9 copy.60
  8.4 1.2 reduce-window.6
  10.1 1.2 fusion.14
  11.3 1.2 fusion.16
  12.6 0.6 broadcast_in_dim.65
  13.2 1.2 reshape.147
  14.4 1.8 convolution_convert_fusion.1
  16.2 19.2 %all_to_all.24 = bf16[4,64,2048]{2,1,0:T(8,128)(2,1)} all-to-all(bf16[4,64,2048]{2,1,0:T(8,128)(2,1)S(1)} %bitcast.83), channel_id=1, replica_groups=mesh['ep'=4,'tp'=8] {'ep'}, dimensions={0} | all-to-all | bytes 2097152 | tf_op jit(solution)/shard_map/all_to_all | solution.py:120
  35.5 81.9 %all-gather.2.cloned.1.call-done = bf16[2048,2048]{1,0:T(8,128)(2,1)} async-done(((bf16[256,2048]{1,0:T(8,128)(2,1)}), bf16[2048,2048]{1,0:T(8,128)(2,1)}) %all-gather.2.cloned.1.call-update) | async-done | bytes 8388624 | tf_op jit(solution)/shard_map/all_gather | solution.py:121
  117.4 7.2 %fusion.10 = f32[2048,448]{0,1:T(8,128)S(1)} fusion(bf16[2048,2048]{1,0:T(8,128)(2,1)} %all-gather.2.cloned.1.call-done, bf16[1,2048,448]{1,2,0:T(8,128)(2,1)} %param.27), kind=kOutput, calls=%fused_computation.22 | convolution fusion | flops 3758096384 | bytes 13893632 | tf_op jit(solution)/shard_map/dot_general | solution.py:122
  124.6 4.3 %multiply_convert_fusion = bf16[2048,448]{0,1:T(8,128)(2,1)S(1)} fusion(f32[2048,448]{0,1:T(8,128)S(1)} %fusion.10, bf16[2048,2048]{1,0:T(8,128)(2,1)S(1)} %copy-done.8, bf16[1,2048,448]{1,2,0:T(8,128)(2,1)S(1)} %copy-done.9), kind=kOutput, calls=%fused_computation.16 | convolution fusion | flops 3763601408 | bytes 15728640 | tf_op jit(solution)/shard_map/dot_general | solution.py:123
  128.9 6.9 %convolution_convert_fusion = bf16[2048,2048]{1,0:T(8,128)(2,1)} fusion(bf16[2048,448]{0,1:T(8,128)(2,1)S(1)} %multiply_convert_fusion, bf16[1,448,2048]{2,1,0:T(8,128)(2,1)S(1)} %copy-done), kind=kOutput, calls=%fused_computation.15 | convolution fusion | flops 3762290688 | bytes 12058624 | tf_op jit(solution)/shard_map/dot_general | solution.py:127
  136.1 0.5 copy-done.1
  138.0 4.4 %reduce_window_sum.35 = f32[4,128,128]{1,2,0:T(8,128)S(1)} reduce-window(f32[4,128,128]{1,2,0:T(8,128)S(1)} %get-tuple-element.197, f32[]{:T(128)} %constant.53.clone.1), window={size=1x1x128 pad=0_0x0_0x0_127}, to_apply=%region_2.3 | reduce-window | flops 8323072 | bytes 524292 | tf_op jit(solution)/shard_map/absorb/reduce_window_sum | solution.py:33
  142.8 36.9 %while.19 = (s32[]{:T(128)}, bf16[128,256]{0,1:T(8,128)(2,1)S(1)}, bf16[128,256]{0,1:T(8,128)(2,1)S(1)}, f32[128,4,64]{0,2,1:T(8,128)S(1)}, f32[4,128]{1,0:T(4,1...) while((s32[]{:T(128)}, bf16[128,256]{0,1:T(8,128)(2,1)S(1)}, ...), condition=%wide.region_7.8_spmd, body=%wide.region_4.7_spmd.sunk | while | flops 27738116 | bytes 3139796 | solution.py:95
  142.8 3.4 %collective-permute-start = (bf16[128,256]{0,1:T(8,128)(2,1)S(1)}, bf16[128,256]{0,1:T(8,128)(2,1)S(1)}, u32[]{:S(2)}, u32[]{:S(2)}) collective-permute-start(bf16[128,256]{0,1:T(8,128)(2,1)S(1)} %get-tuple-element.268), channel_id=1, source_target_pairs={{0,8},{8,16},{16,24},{1,9},{9,17},{17,25},{2,10},{10,18},{18,26},{... | collective-permute-start | bytes 196616 | tf_op jit(solution)/shard_map/while/body/eval_jaxpr/ppermute | solution.py:14
  146.1 3.4 %collective-permute-start.1 = (bf16[128,256]{0,1:T(8,128)(2,1)S(1)}, bf16[128,256]{0,1:T(8,128)(2,1)S(1)}, u32[]{:S(2)}, u32[]{:S(2)}) collective-permute-start(bf16[128,256]{0,1:T(8,128)(2,1)S(1)} %get-tuple-element.269), channel_id=1, source_target_pairs={{0,8},{8,16},{16,24},{1,9},{9,17},{17,25},{2,10},{10,18},{18,26},{... | collective-permute-start | bytes 196616 | tf_op jit(solution)/shard_map/while/body/eval_jaxpr/ppermute | solution.py:14
  150.0 4.4 %reduce_window_sum.40 = f32[4,128,128]{1,2,0:T(8,128)S(1)} reduce-window(f32[4,128,128]{1,2,0:T(8,128)S(1)} %get-tuple-element.255, f32[]{:T(128)} %constant.53.clone.1..sunk), window={size=1x1x128 pad=0_0x0_0x0_127}, to_apply=%region_5.5 | reduce-window | flops 8323072 | bytes 524292 | tf_op jit(solution)/shard_map/while/body/eval_jaxpr/reduce_window_sum | solution.py:33
  154.5 0.4 fusion.57
  154.9 3.4 %collective-permute-start = (bf16[128,256]{0,1:T(8,128)(2,1)S(1)}, bf16[128,256]{0,1:T(8,128)(2,1)S(1)}, u32[]{:S(2)}, u32[]{:S(2)}) collective-permute-start(bf16[128,256]{0,1:T(8,128)(2,1)S(1)} %get-tuple-element.268), channel_id=1, source_target_pairs={{0,8},{8,16},{16,24},{1,9},{9,17},{17,25},{2,10},{10,18},{18,26},{... | collective-permute-start | bytes 196616 | tf_op jit(solution)/shard_map/while/body/eval_jaxpr/ppermute | solution.py:14
  158.3 3.6 %collective-permute-start.1 = (bf16[128,256]{0,1:T(8,128)(2,1)S(1)}, bf16[128,256]{0,1:T(8,128)(2,1)S(1)}, u32[]{:S(2)}, u32[]{:S(2)}) collective-permute-start(bf16[128,256]{0,1:T(8,128)(2,1)S(1)} %get-tuple-element.269), channel_id=1, source_target_pairs={{0,8},{8,16},{16,24},{1,9},{9,17},{17,25},{2,10},{10,18},{18,26},{... | collective-permute-start | bytes 196616 | tf_op jit(solution)/shard_map/while/body/eval_jaxpr/ppermute | solution.py:14
  162.4 4.4 %reduce_window_sum.40 = f32[4,128,128]{1,2,0:T(8,128)S(1)} reduce-window(f32[4,128,128]{1,2,0:T(8,128)S(1)} %get-tuple-element.255, f32[]{:T(128)} %constant.53.clone.1..sunk), window={size=1x1x128 pad=0_0x0_0x0_127}, to_apply=%region_5.5 | reduce-window | flops 8323072 | bytes 524292 | tf_op jit(solution)/shard_map/while/body/eval_jaxpr/reduce_window_sum | solution.py:33
  166.9 0.4 fusion.57
  167.3 2.5 collective-permute-start
  169.8 4.5 %collective-permute-start.1 = (bf16[128,256]{0,1:T(8,128)(2,1)S(1)}, bf16[128,256]{0,1:T(8,128)(2,1)S(1)}, u32[]{:S(2)}, u32[]{:S(2)}) collective-permute-start(bf16[128,256]{0,1:T(8,128)(2,1)S(1)} %get-tuple-element.269), channel_id=1, source_target_pairs={{0,8},{8,16},{16,24},{1,9},{9,17},{17,25},{2,10},{10,18},{18,26},{... | collective-permute-start | bytes 196616 | tf_op jit(solution)/shard_map/while/body/eval_jaxpr/ppermute | solution.py:14
  174.8 4.4 %reduce_window_sum.40 = f32[4,128,128]{1,2,0:T(8,128)S(1)} reduce-window(f32[4,128,128]{1,2,0:T(8,128)S(1)} %get-tuple-element.255, f32[]{:T(128)} %constant.53.clone.1..sunk), window={size=1x1x128 pad=0_0x0_0x0_127}, to_apply=%region_5.5 | reduce-window | flops 8323072 | bytes 524292 | tf_op jit(solution)/shard_map/while/body/eval_jaxpr/reduce_window_sum | solution.py:33
  179.8 2.4 convolution_convert_fusion.2
  182.1 41.8 %reduce-scatter.5.cloned.1.call-done = bf16[256,2048]{1,0:T(8,128)(2,1)} async-done(((bf16[2048,2048]{1,0:T(8,128)(2,1)}), bf16[256,2048]{1,0:T(8,128)(2,1)}) %reduce-scatter.5.cloned.1.call-update) | async-done | bytes 1048592 | tf_op jit(solution)/shard_map/reduce_scatter | solution.py:126
  223.9 3.7 %all-to-all-start.1 = ((bf16[4,64,2048]{2,1,0:T(8,128)(2,1)}), bf16[4,64,2048]{2,1,0:T(8,128)(2,1)S(1)}, u32[]{:S(2)}, u32[]{:S(2)}) async-start(bf16[4,64,2048]{2,1,0:T(8,128)(2,1)} %bitcast.86), calls=%async_computation.3 | async-start | bytes 2097152 | tf_op jit(solution)/shard_map/all_to_all | solution.py:132
  227.9 11.7 %all-to-all-done.1 = bf16[4,64,2048]{2,1,0:T(8,128)(2,1)S(1)} async-done(((bf16[4,64,2048]{2,1,0:T(8,128)(2,1)}), bf16[4,64,2048]{2,1,0:T(8,128)(2,1)S(1)}, u32[]{:S(2)}, u32[]{:S(2)}) %all-to-all-start.1) | async-done | bytes 1048608 | tf_op jit(solution)/shard_map/all_to_all | solution.py:132
  239.6 1.3 fusion.12
  241.0 15.6 %reduce-scatter.3.cloned.1.call-done = bf16[16,2048]{1,0:T(8,128)(2,1)} async-done(((bf16[128,2048]{1,0:T(8,128)(2,1)}), bf16[16,2048]{1,0:T(8,128)(2,1)}) %reduce-scatter.3.cloned.1.call-update) | async-done | bytes 65552 | tf_op jit(solution)/shard_map/reduce_scatter | solution.py:42
  (82 shorter events, 4.8 us)
Async XLA Ops:
  7.2 121.7 %copy-start = (bf16[1,448,2048]{2,1,0:T(8,128)(2,1)S(1)}, bf16[1,448,2048]{2,1,0:T(8,128)(2,1)}, u32[]{:S(2)}) copy-start(bf16[1,448,2048]{2,1,0:T(8,128)(2,1)} %param.29) | copy-start | bytes 5505028
  7.2 110.2 %all-gather.2.cloned.1.call-start = ((), (), s32[]{:S(2)}) async-start(), calls=%async_computation.5 | async-start | bytes 9437184 | tf_op jit(solution)/shard_map/all_gather | solution.py:121
  35.5 188.5 %reduce-scatter.5.cloned.1.call-start = ((), (), s32[]{:S(2)}) async-start(), calls=%async_computation.6 | async-start | bytes 9437184 | tf_op jit(solution)/shard_map/reduce_scatter | solution.py:126
  117.4 7.2 %copy-start.8 = (bf16[2048,2048]{1,0:T(8,128)(2,1)S(1)}, bf16[2048,2048]{1,0:T(8,128)(2,1)}, u32[]{:S(2)}) copy-start(bf16[2048,2048]{1,0:T(8,128)(2,1)} %all-gather.2.cloned.1.call-done) | copy-start | bytes 25165828
  117.4 7.2 %copy-start.9 = (bf16[1,2048,448]{1,2,0:T(8,128)(2,1)S(1)}, bf16[1,2048,448]{1,2,0:T(8,128)(2,1)}, u32[]{:S(2)}) copy-start(bf16[1,2048,448]{1,2,0:T(8,128)(2,1)} %param.28) | copy-start | bytes 5505028
  135.8 0.8 copy-start.1
  135.8 0.9 copy-start.2
  135.8 1.1 copy-start.3
  135.8 1.2 copy-start.7
  135.8 1.5 copy-start.6
  135.8 1.6 copy-start.10
  135.8 120.7 %reduce-scatter.3.cloned.1.call-start = ((), (), s32[]{:S(2)}) async-start(), calls=%async_computation.4 | async-start | bytes 589824 | tf_op jit(solution)/shard_map/reduce_scatter | solution.py:42
  142.8 6.8 %collective-permute-start = (bf16[128,256]{0,1:T(8,128)(2,1)S(1)}, bf16[128,256]{0,1:T(8,128)(2,1)S(1)}, u32[]{:S(2)}, u32[]{:S(2)}) collective-permute-start(bf16[128,256]{0,1:T(8,128)(2,1)S(1)} %get-tuple-element.268), channel_id=1, source_target_pairs={{0,8},{8,16},{16,24},{1,9},{9,17},{17,25},{2,10},{10,18},{18,26},{... | collective-permute-start | bytes 196616 | tf_op jit(solution)/shard_map/while/body/eval_jaxpr/ppermute | solution.py:14
  146.1 8.3 %collective-permute-start.1 = (bf16[128,256]{0,1:T(8,128)(2,1)S(1)}, bf16[128,256]{0,1:T(8,128)(2,1)S(1)}, u32[]{:S(2)}, u32[]{:S(2)}) collective-permute-start(bf16[128,256]{0,1:T(8,128)(2,1)S(1)} %get-tuple-element.269), channel_id=1, source_target_pairs={{0,8},{8,16},{16,24},{1,9},{9,17},{17,25},{2,10},{10,18},{18,26},{... | collective-permute-start | bytes 196616 | tf_op jit(solution)/shard_map/while/body/eval_jaxpr/ppermute | solution.py:14
  154.9 7.0 %collective-permute-start = (bf16[128,256]{0,1:T(8,128)(2,1)S(1)}, bf16[128,256]{0,1:T(8,128)(2,1)S(1)}, u32[]{:S(2)}, u32[]{:S(2)}) collective-permute-start(bf16[128,256]{0,1:T(8,128)(2,1)S(1)} %get-tuple-element.268), channel_id=1, source_target_pairs={{0,8},{8,16},{16,24},{1,9},{9,17},{17,25},{2,10},{10,18},{18,26},{... | collective-permute-start | bytes 196616 | tf_op jit(solution)/shard_map/while/body/eval_jaxpr/ppermute | solution.py:14
  158.3 8.6 %collective-permute-start.1 = (bf16[128,256]{0,1:T(8,128)(2,1)S(1)}, bf16[128,256]{0,1:T(8,128)(2,1)S(1)}, u32[]{:S(2)}, u32[]{:S(2)}) collective-permute-start(bf16[128,256]{0,1:T(8,128)(2,1)S(1)} %get-tuple-element.269), channel_id=1, source_target_pairs={{0,8},{8,16},{16,24},{1,9},{9,17},{17,25},{2,10},{10,18},{18,26},{... | collective-permute-start | bytes 196616 | tf_op jit(solution)/shard_map/while/body/eval_jaxpr/ppermute | solution.py:14
  167.3 7.0 %collective-permute-start = (bf16[128,256]{0,1:T(8,128)(2,1)S(1)}, bf16[128,256]{0,1:T(8,128)(2,1)S(1)}, u32[]{:S(2)}, u32[]{:S(2)}) collective-permute-start(bf16[128,256]{0,1:T(8,128)(2,1)S(1)} %get-tuple-element.268), channel_id=1, source_target_pairs={{0,8},{8,16},{16,24},{1,9},{9,17},{17,25},{2,10},{10,18},{18,26},{... | collective-permute-start | bytes 196616 | tf_op jit(solution)/shard_map/while/body/eval_jaxpr/ppermute | solution.py:14
  169.8 9.5 %collective-permute-start.1 = (bf16[128,256]{0,1:T(8,128)(2,1)S(1)}, bf16[128,256]{0,1:T(8,128)(2,1)S(1)}, u32[]{:S(2)}, u32[]{:S(2)}) collective-permute-start(bf16[128,256]{0,1:T(8,128)(2,1)S(1)} %get-tuple-element.269), channel_id=1, source_target_pairs={{0,8},{8,16},{16,24},{1,9},{9,17},{17,25},{2,10},{10,18},{18,26},{... | collective-permute-start | bytes 196616 | tf_op jit(solution)/shard_map/while/body/eval_jaxpr/ppermute | solution.py:14
  179.7 48.2 %copy-start.5 = (f32[128,2]{0,1:T(2,128)S(1)}, f32[128,2]{0,1:T(2,128)}, u32[]{:S(2)}) copy-start(f32[128,2]{0,1:T(2,128)} %param.26) | copy-start | bytes 3076
  179.7 48.2 %copy-start.4 = (s32[128,2]{0,1:T(2,128)S(1)}, s32[128,2]{0,1:T(2,128)}, u32[]{:S(2)}) copy-start(s32[128,2]{0,1:T(2,128)} %param.25) | copy-start | bytes 3076
  223.9 15.7 %all-to-all-start.1 = ((bf16[4,64,2048]{2,1,0:T(8,128)(2,1)}), bf16[4,64,2048]{2,1,0:T(8,128)(2,1)S(1)}, u32[]{:S(2)}, u32[]{:S(2)}) async-start(bf16[4,64,2048]{2,1,0:T(8,128)(2,1)} %bitcast.86), calls=%async_computation.3 | async-start | bytes 2097152 | tf_op jit(solution)/shard_map/all_to_all | solution.py:132
Sparse Core Ops, SparseCore 0:
  35.6 81.7 all-gather.1
  136.0 87.9 reduce-scatter.4
  226.8 29.7 reduce-scatter.2
where the time goes:
time: 264 us; the launch traced here: 263 us
  waiting for transfers between devices  151 us (57%)
  matrix products  26.4 us (10%)
  starting transfers between devices  24.8 us (9%)
  other arithmetic  22.8 us (9%)
  blocking collectives  19.2 us (7%)
  between operations  14 us (5%)
  local copies, waits for them, and re-layouts  4.56 us (2%)
    all_gather x1, waiting for transfers between devices, body(): piece = lax.all_gather(arrived, 'tp', axis=0, tiled=True)  81.9 us
    reduce_scatter x1, waiting for transfers between devices, body(): lax.psum_scatter(jnp.dot(hidden, down_local, preferred_element_type=jnp.f...  41.8 us
    ppermute x6, starting transfers between devices, shifted(): return lax.ppermute(array, axis, pairs)  20.8 us
    all_to_all x1, blocking collectives, body(): lax.all_to_all(outgoing, 'ep', split_axis=0, concat_axis=0, tiled=True)  19.2 us
    another operation x4, other arithmetic, absorb(): lax.cumsum(log_fail, axis=2, reverse=True)  17.7 us
    reduce_scatter x1, waiting for transfers between devices, mixer_reduce(): lax.psum_scatter(jnp.dot(heads_mixed, mixer_out_weight, preferred_element...  15.6 us
    all_to_all x1, waiting for transfers between devices, body(): lax.all_to_all(expert_sum, 'ep', split_axis=0, concat_axis=0, tiled=True)  11.7 us
    dot_general x1, matrix products, body(): gate_piece = jnp.dot(piece, gate_local, preferred_element_type=jnp.float32)  7.17 us
  transfers between devices with their start and end apart: 10, of which 4 were waited for; matrix products, arithmetic and copies ran while one was open for 10% of the time, Pallas kernels for 0%

commit v1 on v0

--- a/solution.py
+++ b/solution.py
@@ -118,7 +118,12 @@
         jnp.bfloat16
     )
     arrived = lax.all_to_all(outgoing, "ep", split_axis=0, concat_axis=0, tiled=True)
-    piece = lax.all_gather(arrived, "tp", axis=0, tiled=True)
+    ring = [arrived]
+    for hop in range(7):
+        ring.append(lax.ppermute(ring[-1], "tp", [(dev, (dev + 1) % 8) for dev in range(8)]))
+    piece = jnp.roll(
+        jnp.concatenate(ring[::-1], axis=0), (lax.axis_index("tp") + 1) * ring[0].shape[0], axis=0
+    )
     gate_piece = jnp.dot(piece, gate_local, preferred_element_type=jnp.float32)
     up_piece = jnp.dot(piece, up_local, preferred_element_type=jnp.float32)
     hidden = (jax.nn.silu(gate_piece) * up_piece).astype(jnp.bfloat16)

time: 264 us -> 318 us (1.20)
  waiting for transfers between devices: 151 us -> 181 us
  local copies, waits for them, and re-layouts: 4.56 us -> 26.8 us
    ppermute x0 -> x7, waiting for transfers between devices: none -> 113 us  [body(): lax.ppermute(ring[-1], 'tp', [(dev, (dev + 1) % 8) for dev in range(8)])]
    all_gather x1 -> x0, waiting for transfers between devices: 81.9 us -> none  [body(): piece = lax.all_gather(arrived, 'tp', axis=0, tiled=True)]
    unnamed x24 -> x59, local copies, waits for them, and re-layouts: 1.62 us -> 23.8 us
    dot_general x1, matrix products: 6.89 us -> 14.3 us  [body(): jnp.dot(hidden, down_local, preferred_element_type=jnp.float32)]
    dot_general x1 -> x0, matrix products: 7.17 us -> none  [body(): gate_piece = jnp.dot(piece, gate_local, preferred_element_type=jnp.float32)]
  transfers between devices with their start and end apart: 10 -> 16, of which waited for: 4 -> 10; matrix products, arithmetic and copies ran while one was open for 10% -> 8% of each run, Pallas kernels for 0% -> 0%
where the time goes in v1:
time: 318 us; the launch traced here: 317 us
  waiting for transfers between devices  181 us (57%)
  matrix products  28.3 us (9%)
  local copies, waits for them, and re-layouts  26.8 us (8%)
  starting transfers between devices  24.2 us (8%)
  other arithmetic  22.8 us (7%)
  blocking collectives  19.1 us (6%)
  between operations  14.5 us (5%)
    ppermute x7, waiting for transfers between devices, body(): lax.ppermute(ring[-1], 'tp', [(dev, (dev + 1) % 8) for dev in range(8)])  113 us
    reduce_scatter x1, waiting for transfers between devices, body(): lax.psum_scatter(jnp.dot(hidden, down_local, preferred_element_type=jnp.f...  41.1 us
    unnamed x59, local copies, waits for them, and re-layouts  23.8 us
    ppermute x6, starting transfers between devices, shifted(): return lax.ppermute(array, axis, pairs)  20.2 us
    all_to_all x1, blocking collectives, body(): lax.all_to_all(outgoing, 'ep', split_axis=0, concat_axis=0, tiled=True)  19.1 us
    another operation x4, other arithmetic, absorb(): lax.cumsum(log_fail, axis=2, reverse=True)  17.7 us
    reduce_scatter x1, waiting for transfers between devices, mixer_reduce(): lax.psum_scatter(jnp.dot(heads_mixed, mixer_out_weight, preferred_element...  15.9 us
    dot_general x1, matrix products, body(): jnp.dot(hidden, down_local, preferred_element_type=jnp.float32)  14.3 us
  transfers between devices with their start and end apart: 16, of which 10 were waited for; matrix products, arithmetic and copies ran while one was open for 8% of the time, Pallas kernels for 0%

profile of v1, /device:TPU:0, one launch (start us, length us, event | category | flops | bytes accessed | tf_op | source)
XLA Modules:
  0.0 317.1 jit_solution(951845238459855287)
XLA Ops:
  14.4 1.8 convolution_convert_fusion.1
  16.2 19.1 %all_to_all.24 = bf16[4,64,2048]{2,1,0:T(8,128)(2,1)S(1)} all-to-all(bf16[4,64,2048]{2,1,0:T(8,128)(2,1)S(1)} %bitcast.83), channel_id=1, replica_groups=mesh['ep'=4,'tp'=8] {'ep'}, dimensions={0} | all-to-all | bytes 2097152 | tf_op jit(solution)/shard_map/all_to_all | solution.py:120
  35.4 16.0 %collective-permute-done.2 = bf16[256,2048]{1,0:T(8,128)(2,1)S(1)} collective-permute-done((bf16[256,2048]{1,0:T(8,128)(2,1)S(1)}, bf16[256,2048]{1,0:T(8,128)(2,1)S(1)}, u32[]{:S(2)}, u32[]{:S(2)}) %collective-permute-start.2) | collective-permute-done | bytes 1048608 | tf_op jit(solution)/shard_map/ppermute | solution.py:123
  52.4 16.0 %collective-permute-done.3 = bf16[256,2048]{1,0:T(8,128)(2,1)S(1)} collective-permute-done((bf16[256,2048]{1,0:T(8,128)(2,1)S(1)}, bf16[256,2048]{1,0:T(8,128)(2,1)S(1)}, u32[]{:S(2)}, u32[]{:S(2)}) %collective-permute-start.3) | collective-permute-done | bytes 1048608 | tf_op jit(solution)/shard_map/ppermute | solution.py:123
  69.4 16.0 %collective-permute-done.4 = bf16[256,2048]{1,0:T(8,128)(2,1)S(1)} collective-permute-done((bf16[256,2048]{1,0:T(8,128)(2,1)S(1)}, bf16[256,2048]{1,0:T(8,128)(2,1)S(1)}, u32[]{:S(2)}, u32[]{:S(2)}) %collective-permute-start.4) | collective-permute-done | bytes 1048608 | tf_op jit(solution)/shard_map/ppermute | solution.py:123
  86.4 16.0 %collective-permute-done.5 = bf16[256,2048]{1,0:T(8,128)(2,1)S(1)} collective-permute-done((bf16[256,2048]{1,0:T(8,128)(2,1)S(1)}, bf16[256,2048]{1,0:T(8,128)(2,1)S(1)}, u32[]{:S(2)}, u32[]{:S(2)}) %collective-permute-start.5) | collective-permute-done | bytes 1048608 | tf_op jit(solution)/shard_map/ppermute | solution.py:123
  103.4 16.0 %collective-permute-done.6 = bf16[256,2048]{1,0:T(8,128)(2,1)S(1)} collective-permute-done((bf16[256,2048]{1,0:T(8,128)(2,1)S(1)}, bf16[256,2048]{1,0:T(8,128)(2,1)S(1)}, u32[]{:S(2)}, u32[]{:S(2)}) %collective-permute-start.6) | collective-permute-done | bytes 1048608 | tf_op jit(solution)/shard_map/ppermute | solution.py:123
  120.4 16.1 %collective-permute-done.7 = bf16[256,2048]{1,0:T(8,128)(2,1)} collective-permute-done((bf16[256,2048]{1,0:T(8,128)(2,1)S(1)}, bf16[256,2048]{1,0:T(8,128)(2,1)}, u32[]{:S(2)}, u32[]{:S(2)}) %collective-permute-start.7) | collective-permute-done | bytes 1048608 | tf_op jit(solution)/shard_map/ppermute | solution.py:123
  136.6 16.3 %collective-permute-done.8 = bf16[256,2048]{1,0:T(8,128)(2,1)} collective-permute-done((bf16[256,2048]{1,0:T(8,128)(2,1)}, bf16[256,2048]{1,0:T(8,128)(2,1)}, u32[]{:S(2)}, u32[]{:S(2)}) %collective-permute-start.8) | collective-permute-done | bytes 1048608 | tf_op jit(solution)/shard_map/ppermute | solution.py:123
  155.5 1.3 constant_dynamic-update-slice_fusion.13
  158.1 1.3 constant_dynamic-update-slice_fusion.11
  159.4 1.3 constant_dynamic-update-slice_fusion.10
  165.2 5.7 %copy-done.12 = bf16[4096,2048]{1,0:T(8,128)(2,1)} copy-done((bf16[4096,2048]{1,0:T(8,128)(2,1)}, bf16[4096,2048]{1,0:T(8,128)(2,1)S(1)}, u32[]{:S(2)}) %copy-start.12) | copy-done | bytes 16777240
  170.9 5.9 %fusion.8 = f32[2048,448]{0,1:T(8,128)} fusion(bf16[4096,2048]{1,0:T(8,128)(2,1)S(1)} %constant_dynamic-update-slice_fusion, s32[]{:T(128)S(6)} %select_n.50, bf16[1,2048,448]{1,2,0:T(8,128)(2,1)S(1)} %copy-done.19), kind=kOutput, calls=%fused_computation.16 | convolution fusion | flops 3758096384 | bytes 13893636 | tf_op jit(solution)/shard_map/dot_general | solution.py:128
  176.8 14.3 %convolution_convert_fusion = bf16[2048,2048]{1,0:T(8,128)(2,1)} fusion(f32[2048,448]{0,1:T(8,128)} %fusion.8, bf16[1,448,2048]{2,1,0:T(8,128)(2,1)S(1)} %copy-done, bf16[4096,2048]{1,0:T(8,128)(2,1)} %copy-done.12, s32[]{:T(128)S(6)} %select_n.50, bf16[1,2048,448]{1,2,0:T(8,128)(2,1)} %param.27), kind=kOutput, calls=%fused_computation.15 | convolution fusion | flops 7525892096 | bytes 24117252 | tf_op jit(solution)/shard_map/dot_general | solution.py:132
  192.8 4.4 %reduce_window_sum.35 = f32[4,128,128]{1,2,0:T(8,128)S(1)} reduce-window(f32[4,128,128]{1,2,0:T(8,128)S(1)} %get-tuple-element.197, f32[]{:T(128)} %constant.74.clone.1), window={size=1x1x128 pad=0_0x0_0x0_127}, to_apply=%region_2.3 | reduce-window | flops 8323072 | bytes 524292 | tf_op jit(solution)/shard_map/absorb/reduce_window_sum | solution.py:33
  197.6 36.4 %while.19 = (s32[]{:T(128)}, bf16[128,256]{0,1:T(8,128)(2,1)S(1)}, bf16[128,256]{0,1:T(8,128)(2,1)S(1)}, f32[128,4,64]{0,2,1:T(8,128)S(1)}, f32[4,128]{1,0:T(4,1...) while((s32[]{:T(128)}, bf16[128,256]{0,1:T(8,128)(2,1)S(1)}, ...), condition=%wide.region_7.8_spmd, body=%wide.region_4.7_spmd.sunk | while | flops 27738116 | bytes 3139796 | solution.py:95
  197.6 2.8 collective-permute-start
  200.4 3.4 %collective-permute-start.1 = (bf16[128,256]{0,1:T(8,128)(2,1)S(1)}, bf16[128,256]{0,1:T(8,128)(2,1)S(1)}, u32[]{:S(2)}, u32[]{:S(2)}) collective-permute-start(bf16[128,256]{0,1:T(8,128)(2,1)S(1)} %get-tuple-element.269), channel_id=1, source_target_pairs={{0,8},{8,16},{16,24},{1,9},{9,17},{17,25},{2,10},{10,18},{18,26},{... | collective-permute-start | bytes 196616 | tf_op jit(solution)/shard_map/while/body/eval_jaxpr/ppermute | solution.py:14
  204.3 4.4 %reduce_window_sum.40 = f32[4,128,128]{1,2,0:T(8,128)S(1)} reduce-window(f32[4,128,128]{1,2,0:T(8,128)S(1)} %get-tuple-element.255, f32[]{:T(128)} %constant.74.clone.1..sunk), window={size=1x1x128 pad=0_0x0_0x0_127}, to_apply=%region_5.5 | reduce-window | flops 8323072 | bytes 524292 | tf_op jit(solution)/shard_map/while/body/eval_jaxpr/reduce_window_sum | solution.py:33
  209.2 3.4 %collective-permute-start = (bf16[128,256]{0,1:T(8,128)(2,1)S(1)}, bf16[128,256]{0,1:T(8,128)(2,1)S(1)}, u32[]{:S(2)}, u32[]{:S(2)}) collective-permute-start(bf16[128,256]{0,1:T(8,128)(2,1)S(1)} %get-tuple-element.268), channel_id=1, source_target_pairs={{0,8},{8,16},{16,24},{1,9},{9,17},{17,25},{2,10},{10,18},{18,26},{... | collective-permute-start | bytes 196616 | tf_op jit(solution)/shard_map/while/body/eval_jaxpr/ppermute | solution.py:14
  212.6 3.6 %collective-permute-start.1 = (bf16[128,256]{0,1:T(8,128)(2,1)S(1)}, bf16[128,256]{0,1:T(8,128)(2,1)S(1)}, u32[]{:S(2)}, u32[]{:S(2)}) collective-permute-start(bf16[128,256]{0,1:T(8,128)(2,1)S(1)} %get-tuple-element.269), channel_id=1, source_target_pairs={{0,8},{8,16},{16,24},{1,9},{9,17},{17,25},{2,10},{10,18},{18,26},{... | collective-permute-start | bytes 196616 | tf_op jit(solution)/shard_map/while/body/eval_jaxpr/ppermute | solution.py:14
  216.7 4.4 %reduce_window_sum.40 = f32[4,128,128]{1,2,0:T(8,128)S(1)} reduce-window(f32[4,128,128]{1,2,0:T(8,128)S(1)} %get-tuple-element.255, f32[]{:T(128)} %constant.74.clone.1..sunk), window={size=1x1x128 pad=0_0x0_0x0_127}, to_apply=%region_5.5 | reduce-window | flops 8323072 | bytes 524292 | tf_op jit(solution)/shard_map/while/body/eval_jaxpr/reduce_window_sum | solution.py:33
  221.6 2.8 collective-permute-start
  224.3 4.3 %collective-permute-start.1 = (bf16[128,256]{0,1:T(8,128)(2,1)S(1)}, bf16[128,256]{0,1:T(8,128)(2,1)S(1)}, u32[]{:S(2)}, u32[]{:S(2)}) collective-permute-start(bf16[128,256]{0,1:T(8,128)(2,1)S(1)} %get-tuple-element.269), channel_id=1, source_target_pairs={{0,8},{8,16},{16,24},{1,9},{9,17},{17,25},{2,10},{10,18},{18,26},{... | collective-permute-start | bytes 196616 | tf_op jit(solution)/shard_map/while/body/eval_jaxpr/ppermute | solution.py:14
  229.1 4.4 %reduce_window_sum.40 = f32[4,128,128]{1,2,0:T(8,128)S(1)} reduce-window(f32[4,128,128]{1,2,0:T(8,128)S(1)} %get-tuple-element.255, f32[]{:T(128)} %constant.74.clone.1..sunk), window={size=1x1x128 pad=0_0x0_0x0_127}, to_apply=%region_5.5 | reduce-window | flops 8323072 | bytes 524292 | tf_op jit(solution)/shard_map/while/body/eval_jaxpr/reduce_window_sum | solution.py:33
  234.0 2.4 convolution_convert_fusion.2
  236.4 41.1 %reduce-scatter.5.cloned.1.call-done = bf16[256,2048]{1,0:T(8,128)(2,1)} async-done(((bf16[2048,2048]{1,0:T(8,128)(2,1)}), bf16[256,2048]{1,0:T(8,128)(2,1)}) %reduce-scatter.5.cloned.1.call-update) | async-done | bytes 1048592 | tf_op jit(solution)/shard_map/reduce_scatter | solution.py:131
  277.5 3.6 %all-to-all-start.1 = ((bf16[4,64,2048]{2,1,0:T(8,128)(2,1)}), bf16[4,64,2048]{2,1,0:T(8,128)(2,1)S(1)}, u32[]{:S(2)}, u32[]{:S(2)}) async-start(bf16[4,64,2048]{2,1,0:T(8,128)(2,1)} %bitcast.86), calls=%async_computation.3 | async-start | bytes 2097152 | tf_op jit(solution)/shard_map/all_to_all | solution.py:137
  281.5 11.6 %all-to-all-done.1 = bf16[4,64,2048]{2,1,0:T(8,128)(2,1)S(1)} async-done(((bf16[4,64,2048]{2,1,0:T(8,128)(2,1)}), bf16[4,64,2048]{2,1,0:T(8,128)(2,1)S(1)}, u32[]{:S(2)}, u32[]{:S(2)}) %all-to-all-start.1) | async-done | bytes 1048608 | tf_op jit(solution)/shard_map/all_to_all | solution.py:137
  293.1 1.3 fusion.21
  294.4 15.9 %reduce-scatter.3.cloned.1.call-done = bf16[16,2048]{1,0:T(8,128)(2,1)} async-done(((bf16[128,2048]{1,0:T(8,128)(2,1)}), bf16[16,2048]{1,0:T(8,128)(2,1)}) %reduce-scatter.3.cloned.1.call-update) | async-done | bytes 65552 | tf_op jit(solution)/shard_map/reduce_scatter | solution.py:42
  (128 shorter events, 25.3 us)
Async XLA Ops:
  7.2 169.6 %copy-start = (bf16[1,448,2048]{2,1,0:T(8,128)(2,1)S(1)}, bf16[1,448,2048]{2,1,0:T(8,128)(2,1)}, u32[]{:S(2)}) copy-start(bf16[1,448,2048]{2,1,0:T(8,128)(2,1)} %param.29) | copy-start | bytes 5505028
  7.2 270.4 %reduce-scatter.5.cloned.1.call-start = ((), (), s32[]{:S(2)}) async-start(), calls=%async_computation.5 | async-start | bytes 9437184 | tf_op jit(solution)/shard_map/reduce_scatter | solution.py:131
  35.3 16.0 %collective-permute-start.2 = (bf16[256,2048]{1,0:T(8,128)(2,1)S(1)}, bf16[256,2048]{1,0:T(8,128)(2,1)S(1)}, u32[]{:S(2)}, u32[]{:S(2)}) collective-permute-start(bf16[256,2048]{1,0:T(8,128)(2,1)S(1)} %bitcast.80), channel_id=1, source_target_pairs={{0,1},{1,2},{2,3},{3,4},{4,5},{5,6},{6,7},{7,0},{8,9},{9,10},{10,1... | collective-permute-start | bytes 3145736 | tf_op jit(solution)/shard_map/ppermute | solution.py:123
  52.4 16.0 %collective-permute-start.3 = (bf16[256,2048]{1,0:T(8,128)(2,1)S(1)}, bf16[256,2048]{1,0:T(8,128)(2,1)S(1)}, u32[]{:S(2)}, u32[]{:S(2)}) collective-permute-start(bf16[256,2048]{1,0:T(8,128)(2,1)S(1)} %collective-permute-done.2), channel_id=1, source_target_pairs={{0,1},{1,2},{2,3},{3,4},{4,5},{5,6},{6,7},{7,0},{8,9},{9,10},{10,1... | collective-permute-start | bytes 3145736 | tf_op jit(solution)/shard_map/ppermute | solution.py:123
  69.4 16.0 %collective-permute-start.4 = (bf16[256,2048]{1,0:T(8,128)(2,1)S(1)}, bf16[256,2048]{1,0:T(8,128)(2,1)S(1)}, u32[]{:S(2)}, u32[]{:S(2)}) collective-permute-start(bf16[256,2048]{1,0:T(8,128)(2,1)S(1)} %collective-permute-done.3), channel_id=1, source_target_pairs={{0,1},{1,2},{2,3},{3,4},{4,5},{5,6},{6,7},{7,0},{8,9},{9,10},{10,1... | collective-permute-start | bytes 3145736 | tf_op jit(solution)/shard_map/ppermute | solution.py:123
  86.4 16.0 %collective-permute-start.5 = (bf16[256,2048]{1,0:T(8,128)(2,1)S(1)}, bf16[256,2048]{1,0:T(8,128)(2,1)S(1)}, u32[]{:S(2)}, u32[]{:S(2)}) collective-permute-start(bf16[256,2048]{1,0:T(8,128)(2,1)S(1)} %collective-permute-done.4), channel_id=1, source_target_pairs={{0,1},{1,2},{2,3},{3,4},{4,5},{5,6},{6,7},{7,0},{8,9},{9,10},{10,1... | collective-permute-start | bytes 3145736 | tf_op jit(solution)/shard_map/ppermute | solution.py:123
  103.4 16.0 %collective-permute-start.6 = (bf16[256,2048]{1,0:T(8,128)(2,1)S(1)}, bf16[256,2048]{1,0:T(8,128)(2,1)S(1)}, u32[]{:S(2)}, u32[]{:S(2)}) collective-permute-start(bf16[256,2048]{1,0:T(8,128)(2,1)S(1)} %collective-permute-done.5), channel_id=1, source_target_pairs={{0,1},{1,2},{2,3},{3,4},{4,5},{5,6},{6,7},{7,0},{8,9},{9,10},{10,1... | collective-permute-start | bytes 3145736 | tf_op jit(solution)/shard_map/ppermute | solution.py:123
  120.4 16.1 %collective-permute-start.7 = (bf16[256,2048]{1,0:T(8,128)(2,1)S(1)}, bf16[256,2048]{1,0:T(8,128)(2,1)}, u32[]{:S(2)}, u32[]{:S(2)}) collective-permute-start(bf16[256,2048]{1,0:T(8,128)(2,1)S(1)} %collective-permute-done.6), channel_id=1, source_target_pairs={{0,1},{1,2},{2,3},{3,4},{4,5},{5,6},{6,7},{7,0},{8,9},{9,10},{10,1... | collective-permute-start | bytes 3145736 | tf_op jit(solution)/shard_map/ppermute | solution.py:123
  136.6 16.3 %collective-permute-start.8 = (bf16[256,2048]{1,0:T(8,128)(2,1)}, bf16[256,2048]{1,0:T(8,128)(2,1)}, u32[]{:S(2)}, u32[]{:S(2)}) collective-permute-start(bf16[256,2048]{1,0:T(8,128)(2,1)} %collective-permute-done.7), channel_id=1, source_target_pairs={{0,1},{1,2},{2,3},{3,4},{4,5},{5,6},{6,7},{7,0},{8,9},{9,10},{10,1... | collective-permute-start | bytes 3145736 | tf_op jit(solution)/shard_map/ppermute | solution.py:123
  136.6 28.1 %copy-start.10 = (bf16[256,2048]{1,0:T(8,128)(2,1)S(1)}, bf16[256,2048]{1,0:T(8,128)(2,1)}, u32[]{:S(2)}) copy-start(bf16[256,2048]{1,0:T(8,128)(2,1)} %copy-done.9) | copy-start | bytes 3145732
  136.6 28.2 %copy-start.8 = (bf16[256,2048]{1,0:T(8,128)(2,1)S(1)}, bf16[256,2048]{1,0:T(8,128)(2,1)}, u32[]{:S(2)}) copy-start(bf16[256,2048]{1,0:T(8,128)(2,1)} %copy-done.7) | copy-start | bytes 3145732
  136.6 28.3 %copy-start.6 = (bf16[256,2048]{1,0:T(8,128)(2,1)S(1)}, bf16[256,2048]{1,0:T(8,128)(2,1)}, u32[]{:S(2)}) copy-start(bf16[256,2048]{1,0:T(8,128)(2,1)} %copy-done.5) | copy-start | bytes 3145732
  136.6 28.4 %copy-start.4 = (bf16[256,2048]{1,0:T(8,128)(2,1)S(1)}, bf16[256,2048]{1,0:T(8,128)(2,1)}, u32[]{:S(2)}) copy-start(bf16[256,2048]{1,0:T(8,128)(2,1)} %copy-done.3) | copy-start | bytes 3145732
  136.6 28.4 %copy-start.2 = (bf16[256,2048]{1,0:T(8,128)(2,1)S(1)}, bf16[256,2048]{1,0:T(8,128)(2,1)}, u32[]{:S(2)}) copy-start(bf16[256,2048]{1,0:T(8,128)(2,1)} %copy-done.1) | copy-start | bytes 3145732
  136.6 34.3 %copy-start.19 = (bf16[1,2048,448]{1,2,0:T(8,128)(2,1)S(1)}, bf16[1,2048,448]{1,2,0:T(8,128)(2,1)}, u32[]{:S(2)}) copy-start(bf16[1,2048,448]{1,2,0:T(8,128)(2,1)} %param.28) | copy-start | bytes 5505028
  165.2 5.7 %copy-start.12 = (bf16[4096,2048]{1,0:T(8,128)(2,1)}, bf16[4096,2048]{1,0:T(8,128)(2,1)S(1)}, u32[]{:S(2)}) copy-start(bf16[4096,2048]{1,0:T(8,128)(2,1)S(1)} %constant_dynamic-update-slice_fusion) | copy-start | bytes 50331652
  176.8 14.7 %copy-start.11 = (bf16[128,256]{1,0:T(8,128)(2,1)S(1)}, bf16[128,256]{1,0:T(8,128)(2,1)}, u32[]{:S(2)}) copy-start(bf16[128,256]{1,0:T(8,128)(2,1)} %param.16) | copy-start | bytes 196612
  176.8 14.8 %copy-start.13 = (bf16[128,256]{1,0:T(8,128)(2,1)S(1)}, bf16[128,256]{1,0:T(8,128)(2,1)}, u32[]{:S(2)}) copy-start(bf16[128,256]{1,0:T(8,128)(2,1)} %param.17) | copy-start | bytes 196612
  176.8 14.9 %copy-start.14 = (bf16[128,256]{1,0:T(8,128)(2,1)S(1)}, bf16[128,256]{1,0:T(8,128)(2,1)}, u32[]{:S(2)}) copy-start(bf16[128,256]{1,0:T(8,128)(2,1)} %param.18) | copy-start | bytes 196612
  176.8 15.0 %copy-start.18 = (f32[64]{0:T(128)S(1)}, f32[64]{0:T(128)}, u32[]{:S(2)}) copy-start(f32[64]{0:T(128)} %param.20) | copy-start | bytes 772
  176.8 15.3 %copy-start.17 = (f32[64]{0:T(128)S(1)}, f32[64]{0:T(128)}, u32[]{:S(2)}) copy-start(f32[64]{0:T(128)} %param.19) | copy-start | bytes 772
  176.8 15.4 %copy-start.20 = (f32[4]{0:T(128)S(1)}, f32[4]{0:T(128)}, u32[]{:S(2)}) copy-start(f32[4]{0:T(128)} %param.21) | copy-start | bytes 52
  191.1 90.2 %copy-start.16 = (f32[128,2]{0,1:T(2,128)S(1)}, f32[128,2]{0,1:T(2,128)}, u32[]{:S(2)}) copy-start(f32[128,2]{0,1:T(2,128)} %param.26) | copy-start | bytes 3076
  191.1 90.3 %copy-start.15 = (s32[128,2]{0,1:T(2,128)S(1)}, s32[128,2]{0,1:T(2,128)}, u32[]{:S(2)}) copy-start(s32[128,2]{0,1:T(2,128)} %param.25) | copy-start | bytes 3076
  191.2 119.1 %reduce-scatter.3.cloned.1.call-start = ((), (), s32[]{:S(2)}) async-start(), calls=%async_computation.4 | async-start | bytes 589824 | tf_op jit(solution)/shard_map/reduce_scatter | solution.py:42
  197.6 6.2 %collective-permute-start = (bf16[128,256]{0,1:T(8,128)(2,1)S(1)}, bf16[128,256]{0,1:T(8,128)(2,1)S(1)}, u32[]{:S(2)}, u32[]{:S(2)}) collective-permute-start(bf16[128,256]{0,1:T(8,128)(2,1)S(1)} %get-tuple-element.268), channel_id=1, source_target_pairs={{0,8},{8,16},{16,24},{1,9},{9,17},{17,25},{2,10},{10,18},{18,26},{... | collective-permute-start | bytes 196616 | tf_op jit(solution)/shard_map/while/body/eval_jaxpr/ppermute | solution.py:14
  200.4 8.3 %collective-permute-start.1 = (bf16[128,256]{0,1:T(8,128)(2,1)S(1)}, bf16[128,256]{0,1:T(8,128)(2,1)S(1)}, u32[]{:S(2)}, u32[]{:S(2)}) collective-permute-start(bf16[128,256]{0,1:T(8,128)(2,1)S(1)} %get-tuple-element.269), channel_id=1, source_target_pairs={{0,8},{8,16},{16,24},{1,9},{9,17},{17,25},{2,10},{10,18},{18,26},{... | collective-permute-start | bytes 196616 | tf_op jit(solution)/shard_map/while/body/eval_jaxpr/ppermute | solution.py:14
  209.2 7.0 %collective-permute-start = (bf16[128,256]{0,1:T(8,128)(2,1)S(1)}, bf16[128,256]{0,1:T(8,128)(2,1)S(1)}, u32[]{:S(2)}, u32[]{:S(2)}) collective-permute-start(bf16[128,256]{0,1:T(8,128)(2,1)S(1)} %get-tuple-element.268), channel_id=1, source_target_pairs={{0,8},{8,16},{16,24},{1,9},{9,17},{17,25},{2,10},{10,18},{18,26},{... | collective-permute-start | bytes 196616 | tf_op jit(solution)/shard_map/while/body/eval_jaxpr/ppermute | solution.py:14
  212.6 8.6 %collective-permute-start.1 = (bf16[128,256]{0,1:T(8,128)(2,1)S(1)}, bf16[128,256]{0,1:T(8,128)(2,1)S(1)}, u32[]{:S(2)}, u32[]{:S(2)}) collective-permute-start(bf16[128,256]{0,1:T(8,128)(2,1)S(1)} %get-tuple-element.269), channel_id=1, source_target_pairs={{0,8},{8,16},{16,24},{1,9},{9,17},{17,25},{2,10},{10,18},{18,26},{... | collective-permute-start | bytes 196616 | tf_op jit(solution)/shard_map/while/body/eval_jaxpr/ppermute | solution.py:14
  221.6 7.0 %collective-permute-start = (bf16[128,256]{0,1:T(8,128)(2,1)S(1)}, bf16[128,256]{0,1:T(8,128)(2,1)S(1)}, u32[]{:S(2)}, u32[]{:S(2)}) collective-permute-start(bf16[128,256]{0,1:T(8,128)(2,1)S(1)} %get-tuple-element.268), channel_id=1, source_target_pairs={{0,8},{8,16},{16,24},{1,9},{9,17},{17,25},{2,10},{10,18},{18,26},{... | collective-permute-start | bytes 196616 | tf_op jit(solution)/shard_map/while/body/eval_jaxpr/ppermute | solution.py:14
  224.3 9.2 %collective-permute-start.1 = (bf16[128,256]{0,1:T(8,128)(2,1)S(1)}, bf16[128,256]{0,1:T(8,128)(2,1)S(1)}, u32[]{:S(2)}, u32[]{:S(2)}) collective-permute-start(bf16[128,256]{0,1:T(8,128)(2,1)S(1)} %get-tuple-element.269), channel_id=1, source_target_pairs={{0,8},{8,16},{16,24},{1,9},{9,17},{17,25},{2,10},{10,18},{18,26},{... | collective-permute-start | bytes 196616 | tf_op jit(solution)/shard_map/while/body/eval_jaxpr/ppermute | solution.py:14
  277.5 15.5 %all-to-all-start.1 = ((bf16[4,64,2048]{2,1,0:T(8,128)(2,1)}), bf16[4,64,2048]{2,1,0:T(8,128)(2,1)S(1)}, u32[]{:S(2)}, u32[]{:S(2)}) async-start(bf16[4,64,2048]{2,1,0:T(8,128)(2,1)} %bitcast.86), calls=%async_computation.3 | async-start | bytes 2097152 | tf_op jit(solution)/shard_map/all_to_all | solution.py:137
  (5 other events, 5.0 us)
Sparse Core Ops, SparseCore 0:
  191.3 86.2 reduce-scatter.4
  280.4 29.8 reduce-scatter.2
